TPU v7x, 32 devices: a whole 2x2x4 slice. The times are simulated.
32 devices in a mesh: ep: 4 (over y, x), tp: 8 (over z, core).
Axes of the slice: x: 2, y: 2, z: 4, core: 2. Of those that a mesh axis runs over, the one named last changes fastest.
Arguments:
- tokens: bfloat16 [256, 4096], P(('ep', 'tp')), may hold values from -6 to 6
- rec_state: float32 [256, 2048], P('ep', 'tp'), may hold values from -40 to 40
- conv_state: bfloat16 [256, 3, 2048], P('ep', None, 'tp'), may hold values from -6 to 6
- route_ids: int32 [256, 4], P('ep'), may hold values from 0 to 15, all different within a row; in each aligned block of 8 rows (0 to 7, 8 to 15, ...) at most 2 rows name the same one
- route_weights: float32 [256, 4], P(('ep', 'tp')), may hold values from 0.1 to 1
- first_gain: bfloat16 [4096], replicated, may hold values from 0.099609375 to 1.8984375
- proj_input: bfloat16 [4096, 2048], P(None, 'tp'), may hold values from -0.09375 to 0.09375
- proj_gate: bfloat16 [4096, 2048], P(None, 'tp'), may hold values from -0.09375 to 0.09375
- conv_taps: bfloat16 [4, 2048], replicated, may hold values from -1.5 to 1.5
- decay_logit: float32 [2048], replicated, may hold values from 1 to 6
- block_decay: bfloat16 [16, 128, 128], replicated, may hold values from -0.5 to 0.5
- block_input: bfloat16 [16, 128, 128], replicated, may hold values from -0.5 to 0.5
- rec_gain: bfloat16 [2048], replicated, may hold values from 0.099609375 to 1.8984375
- proj_out: bfloat16 [2048, 4096], P('tp'), may hold values from -0.125 to 0.125
- second_gain: bfloat16 [4096], replicated, may hold values from 0.099609375 to 1.8984375
- expert_gate: bfloat16 [16, 4096, 4096], P('ep', None, 'tp'), may hold values from -0.21875 to 0.21875
- expert_up: bfloat16 [16, 4096, 4096], P('ep', None, 'tp'), may hold values from -0.21875 to 0.21875
- expert_down: bfloat16 [16, 4096, 4096], P('ep', 'tp'), may hold values from -0.0234375 to 0.0234375
Outputs:
- result: bfloat16 [256, 4096], P(('ep', 'tp'))
- new_state: float32 [256, 2048], P('ep', 'tp')
- new_conv: bfloat16 [256, 3, 2048], P('ep', None, 'tp')
Inputs may be any that keep to these rules, and one draw needn't show every extreme that they name: `route_ids`: each row names 4 different experts; in the rows of one device (aligned blocks of 8 rows) no expert is named by more than 2 rows, and one is named by exactly 2.
All inputs are finite; a program needn't handle non-finite values.
Results may differ from a plain program's by a relative error of at most 0.025.
Values may be sent and summed in bfloat16 or wider, within the bound.
A program may use at most 128 MiB of HBM per device.

v0:
```python
import jax
import jax.numpy as jnp
from jax import lax
from jax.sharding import PartitionSpec as P

EXPERTS = 16
EPS = 1e-06
CLAMP = 7.0
ALPHA = 1.702
RATE = 8.0


def norm_rows(values, gain):
    scale = lax.rsqrt(jnp.mean(values * values, axis=-1, keepdims=True) + EPS)
    return values * scale * gain.astype(jnp.float32)


def slot_positions(ids, blocks):
    rows, picks = ids.shape
    onehot = (ids[:, :, None] == jnp.arange(EXPERTS, dtype=jnp.int32)).astype(jnp.int32)
    onehot = onehot.reshape(blocks, rows // blocks * picks, EXPERTS)
    before = jnp.cumsum(onehot, axis=1) - onehot
    return jnp.sum(before * onehot, axis=-1).reshape(rows, picks)


def dispatch_rows(slots, rows_in, total):
    hits = (slots[:, :, None] == jnp.arange(total, dtype=jnp.int32)).astype(jnp.bfloat16)
    chooser = jnp.sum(hits, axis=1)
    return jnp.einsum("ns,nd->sd", chooser, rows_in, preferred_element_type=jnp.float32).astype(
        jnp.bfloat16
    )


def run_experts(piece, expert_gate, expert_up, expert_down):
    gate = jnp.einsum("erd,edf->erf", piece, expert_gate, preferred_element_type=jnp.float32)
    upper = jnp.einsum("erd,edf->erf", piece, expert_up, preferred_element_type=jnp.float32)
    clipped = jnp.minimum(gate, CLAMP)
    act = (
        (jnp.clip(upper, -CLAMP, CLAMP) + 1.0) * (clipped * jax.nn.sigmoid(ALPHA * clipped))
    ).astype(jnp.bfloat16)
    return jnp.einsum("erf,efd->erd", act, expert_down, preferred_element_type=jnp.float32)


def per_device(
    tokens,
    rec_state,
    conv_state,
    route_ids,
    route_weights,
    first_gain,
    proj_input,
    proj_gate,
    conv_taps,
    decay_logit,
    block_decay,
    block_input,
    rec_gain,
    proj_out,
    second_gain,
    expert_gate,
    expert_up,
    expert_down,
):
    tp_count = lax.axis_size("tp")
    tp_place = lax.axis_index("tp")
    local_width = proj_input.shape[1]
    seq_count = rec_state.shape[0]
    own_count = tokens.shape[0]
    top_count = route_ids.shape[1]
    capacity = max(2, own_count * top_count // EXPERTS)
    first_channel = tp_place * local_width
    own_values = tokens.astype(jnp.float32)
    normed = norm_rows(own_values, first_gain).astype(jnp.bfloat16)
    piece = lax.all_gather(normed, "tp", axis=0, tiled=True)
    both = jnp.concatenate(
        [
            jnp.dot(piece, proj_input, preferred_element_type=jnp.float32),
            jnp.dot(piece, proj_gate, preferred_element_type=jnp.float32),
        ],
        axis=1,
    )
    joined = both.astype(jnp.bfloat16)
    branch_in = joined[:, :local_width]
    branch_gate = joined[:, local_width:]
    tap_weights = lax.dynamic_slice_in_dim(conv_taps, first_channel, local_width, 1).astype(
        jnp.float32
    )
    conv_values = conv_state.astype(jnp.float32)
    conv_output = tap_weights[-1] * branch_in.astype(jnp.float32)
    for tap in range(conv_state.shape[1]):
        conv_output = conv_output + tap_weights[tap] * conv_values[:, tap]
    new_conv = jnp.concatenate([conv_state[:, 1:], branch_in[:, None, :]], axis=1)
    block_width = block_decay.shape[1]
    local_blocks = local_width // block_width
    decay_mats = lax.dynamic_slice_in_dim(block_decay, tp_place * local_blocks, local_blocks, 0)
    input_mats = lax.dynamic_slice_in_dim(block_input, tp_place * local_blocks, local_blocks, 0)
    blocked = conv_output.astype(jnp.bfloat16).reshape(seq_count, local_blocks, block_width)
    decay_gate = jax.nn.sigmoid(
        jnp.einsum("rnk,nkj->rnj", blocked, decay_mats, preferred_element_type=jnp.float32).reshape(
            seq_count, local_width
        )
    )
    input_gate = jax.nn.sigmoid(
        jnp.einsum("rnk,nkj->rnj", blocked, input_mats, preferred_element_type=jnp.float32).reshape(
            seq_count, local_width
        )
    )
    decay_logits = lax.dynamic_slice_in_dim(decay_logit, first_channel, local_width, 0)
    log_keep = -RATE * decay_gate * jax.nn.softplus(-decay_logits)
    keep_factor = jnp.exp(log_keep)
    fresh_input = jnp.sqrt(-jnp.expm1(2.0 * log_keep)) * input_gate * conv_output
    new_state = keep_factor * rec_state + fresh_input
    hidden = new_state * jax.nn.gelu(branch_gate.astype(jnp.float32))
    squares = jnp.sum(hidden * hidden, axis=1, keepdims=True)
    gain_part = lax.dynamic_slice_in_dim(rec_gain, first_channel, local_width, 0).astype(
        jnp.float32
    )
    partial_value = jnp.dot(
        (hidden * gain_part).astype(jnp.bfloat16), proj_out, preferred_element_type=jnp.float32
    )
    channels = local_width * tp_count
    width_out = proj_out.shape[1]
    own_ids = lax.dynamic_slice_in_dim(route_ids, tp_place * own_count, own_count, 0)
    own_slots = own_ids * capacity + slot_positions(own_ids, 1)
    mix_part, own_squares = (
        lax.psum_scatter(
            partial_value.astype(jnp.bfloat16), "tp", scatter_dimension=0, tiled=True
        ).astype(jnp.float32),
        lax.psum_scatter(
            squares.astype(jnp.bfloat16), "tp", scatter_dimension=0, tiled=True
        ).astype(jnp.float32),
    )
    residual = own_values + mix_part * lax.rsqrt(own_squares / channels + EPS)
    second_normed = norm_rows(residual, second_gain).astype(jnp.bfloat16)
    outgoing = dispatch_rows(own_slots, second_normed, EXPERTS * capacity).reshape(
        EXPERTS, capacity, width_out
    )
    arrived = lax.all_to_all(outgoing, "ep", split_axis=0, concat_axis=1, tiled=True)
    partials = run_experts(
        lax.all_gather(arrived, "tp", axis=1, tiled=True), expert_gate, expert_up, expert_down
    )
    summed_rows = lax.psum_scatter(
        partials.astype(jnp.bfloat16), "tp", scatter_dimension=1, tiled=True
    )
    returned = lax.all_to_all(summed_rows, "ep", split_axis=1, concat_axis=0, tiled=True)
    returned_rows = returned.reshape(EXPERTS * capacity, width_out).astype(jnp.float32)
    slot_hits = (own_slots[:, :, None] == jnp.arange(EXPERTS * capacity, dtype=jnp.int32)).astype(
        jnp.float32
    )
    combine_weights = jnp.sum(slot_hits * route_weights[:, :, None], axis=1)
    expert_mix = jnp.dot(combine_weights, returned_rows, precision=lax.Precision.HIGHEST)
    result = (residual + expert_mix).astype(jnp.bfloat16)
    return (result, new_state, new_conv)


def solution(mesh):
    in_specs = (
        P(("ep", "tp"), None),
        P("ep", "tp"),
        P("ep", None, "tp"),
        P("ep", None),
        P(("ep", "tp"), None),
        P(),
        P(None, "tp"),
        P(None, "tp"),
        P(),
        P(),
        P(),
        P(),
        P(),
        P("tp", None),
        P(),
        P("ep", None, "tp"),
        P("ep", None, "tp"),
        P("ep", "tp", None),
    )
    out_specs = (P(("ep", "tp"), None), P("ep", "tp"), P("ep", None, "tp"))
    return jax.shard_map(
        per_device, mesh=mesh, in_specs=in_specs, out_specs=out_specs, check_vma=False
    )
```

profile of v0, /device:TPU:0, one launch (start us, length us, event | category | flops | bytes accessed | tf_op | source)
XLA Modules:
  0.0 196.3 jit_solution(4809331061785495694)
XLA Ops:
  7.2 0.0 copy-start
  7.2 0.0 reduce-scatter.6.cloned.1.call-start
  7.2 0.8 dynamic-slice_convert_fusion
  8.1 0.7 convert_element_type.98
  8.8 1.0 fusion.17
  9.8 0.9 fusion.19
  10.7 16.5 %all_gather.6 = bf16[64,4096]{1,0:T(8,128)(2,1)S(1)} all-gather(bf16[8,4096]{1,0:T(8,128)(2,1)S(1)} %fusion.19), channel_id=1, replica_groups=mesh['ep'=4,'tp'=8] {'tp'}, dimensions={0}, use_global_device_ids=true | all-gather | bytes 589824 | tf_op jit(solution)/shard_map/all_gather | solution.py:74
  27.2 0.9 convert_element_type.101
  28.1 2.1 %convolution_convert_fusion.4 = bf16[64,256]{1,0:T(8,128)(2,1)S(1)} fusion(bf16[64,4096]{1,0:T(8,128)(2,1)S(1)} %all_gather.6, bf16[4096,256]{1,0:T(8,128)(2,1)} %param.24), kind=kOutput, calls=%fused_computation.22 | convolution fusion | flops 134234112 | bytes 2654208 | tf_op jit(solution)/shard_map/dot_general | solution.py:77
  30.2 1.0 fusion.11
  31.2 1.0 fusion.7
  32.2 0.8 fusion.49
  33.0 0.8 dynamic-slice_convert_fusion.2
  33.8 0.0 copy-done.6
  33.8 0.1 fusion.29
  33.9 0.0 copy-start.5
  33.9 2.2 %multiply_reduce_fusion.1 = (bf16[64]{0:T(256)(128)(2,1)S(1)}, f32[64,256]{1,0:T(8,128)S(1)}) fusion(f32[64,256]{1,0:T(8,128)S(1)} %fusion.29, bf16[64,4096]{1,0:T(8,128)(2,1)S(1)} %all_gather.6, bf16[4096,256]{1,0:T(8,128)(2,1)} %param.25), kind=kOutput, calls=%fused_computation.63 | convolution fusion | flops 134430656 | bytes 2752640 | tf_op jit(solution)/shard_map/dot_general | solution.py:78
  36.1 0.0 copy-start.8
  36.1 0.0 copy-start.7
  36.1 0.0 copy-start.10
  36.1 0.0 copy-start.3
  36.1 0.0 copy-done
  36.1 1.3 convolution_convert_fusion.1
  37.4 0.0 reduce-scatter.6.cloned.1.call-update
  37.4 0.0 all-gather.2.cloned.1.call-start
  37.5 0.1 constant_dynamic-slice_fusion
  37.6 0.1 copy.58
  37.7 0.1 eq.49
  37.7 0.1 fusion.47
  37.8 0.1 reduce_window_sum.11
  37.9 0.2 select_reduce_fusion.1
  38.1 0.1 reshape.160
  38.1 0.1 copy.50
  38.2 0.0 copy-done.10
  38.3 0.6 dynamic-slice
  39.5 17.0 %all-reduce = bf16[64,1]{0,1:T(2,128)(2,1)S(1)} all-reduce(bf16[64,1]{0,1:T(2,128)(2,1)S(1)} %bitcast.97), channel_id=3, replica_groups=mesh['ep'=4,'tp'=8] {'tp'}, use_global_device_ids=true, to_apply=%region_3.4.clone | all-reduce | flops 64 | bytes 256
  56.5 0.1 rsqrt_bitcast_fusion
  56.6 0.1 fusion.48
  56.6 13.2 %reduce-scatter.6.cloned.1.call-done = bf16[8,4096]{1,0:T(8,128)(2,1)} async-done(((bf16[64,4096]{1,0:T(8,128)(2,1)}), bf16[8,4096]{1,0:T(8,128)(2,1)}) %reduce-scatter.6.cloned.1.call-update) | async-done | bytes 65552 | tf_op jit(solution)/shard_map/reduce_scatter | solution.py:126
  69.9 1.1 multiply_reduce_fusion
  71.0 1.1 convolution_convert_fusion.2
  72.1 0.2 reshape.161
  72.3 9.2 %all_to_all.33 = bf16[16,2,4096]{2,1,0:T(2,128)(2,1)S(1)} all-to-all(bf16[16,2,4096]{2,1,0:T(2,128)(2,1)S(1)} %reshape.161), channel_id=1, replica_groups=mesh['ep'=4,'tp'=8] {'ep'}, dimensions={0} | all-to-all | bytes 524288 | tf_op jit(solution)/shard_map/all_to_all | solution.py:138
  81.5 0.2 copy.78
  81.7 0.8 all_to_all.27
  82.5 0.0 all-gather.2.cloned.1.call-update
  82.5 0.2 reduce-scatter.8.cloned.1.call-start
  82.7 26.3 %all-gather.2.cloned.1.call-done = bf16[4,64,4096]{2,1,0:T(8,128)(2,1)} async-done(((bf16[4,8,4096]{2,1,0:T(8,128)(2,1)}), bf16[4,64,4096]{2,1,0:T(8,128)(2,1)}) %all-gather.2.cloned.1.call-update) | async-done | bytes 2097168 | tf_op jit(solution)/shard_map/all_gather | solution.py:140
  109.0 9.5 %convolution_minimum_fusion = f32[4,64,512]{2,1,0:T(8,128)S(1)} fusion(bf16[4,64,4096]{2,1,0:T(8,128)(2,1)} %all-gather.2.cloned.1.call-done, bf16[4,4096,512]{2,1,0:T(8,128)(2,1)} %param.33), kind=kOutput, calls=%fused_computation.5 | convolution fusion | flops 1073872896 | bytes 19398656 | tf_op jit(solution)/shard_map/erd,edf->erf/dot_general | solution.py:35
  118.5 0.0 copy-done.2
  118.6 17.8 %convolution_convert_fusion = bf16[4,64,4096]{2,1,0:T(8,128)(2,1)} fusion(bf16[4,512,4096]{2,1,0:T(8,128)(2,1)} %param.35, bf16[4,64,4096]{2,1,0:T(8,128)(2,1)S(1)} %copy-done.2, bf16[4,4096,512]{2,1,0:T(8,128)(2,1)} %param.34, f32[4,64,512]{2,1,0:T(8,128)S(1)} %convolution_minimum_fusion), kind=kOutput, calls=%fused_computation | convolution fusion | flops 2149711872 | bytes 38273024 | tf_op jit(solution)/shard_map/erf,efd->erd/dot_general | solution.py:41
  136.4 3.2 %copy.56 = bf16[4,64,4096]{2,0,1:T(4,128)(2,1)S(1)} copy(bf16[4,64,4096]{2,1,0:T(8,128)(2,1)} %convolution_convert_fusion) | data formatting | bytes 4194304
  139.6 2.6 %copy.62 = bf16[8,8,4,4096]{3,1,2,0:T(8,128)(2,1)} copy(bf16[8,8,4,4096]{3,2,1,0:T(4,128)(2,1)S(1)} %bitcast.87) | data formatting | bytes 4194304
  142.2 0.0 reduce-scatter.8.cloned.1.call-update
  142.2 35.6 %reduce-scatter.8.cloned.1.call-done = bf16[8,16384]{1,0:T(8,128)(2,1)} async-done(((bf16[64,16384]{1,0:T(8,128)(2,1)}), bf16[8,16384]{1,0:T(8,128)(2,1)}) %reduce-scatter.8.cloned.1.call-update) | async-done | bytes 262160
  177.8 1.8 reshape.166
  179.6 3.5 %all-to-all-start.1 = ((bf16[4,8,4096]{2,0,1:T(4,128)(2,1)}), bf16[4,8,4096]{2,0,1:T(4,128)(2,1)S(1)}, u32[]{:S(2)}, u32[]{:S(2)}) async-start(bf16[4,8,4096]{2,0,1:T(4,128)(2,1)} %bitcast.19), calls=%async_computation.2 | async-start | bytes 524288 | tf_op jit(solution)/shard_map/all_to_all | solution.py:145
  183.1 0.0 slice-done
  183.1 0.7 pad_maximum_fusion
  183.8 0.1 select_reduce_fusion
  183.9 4.6 %all-to-all-done.1 = bf16[4,8,4096]{2,0,1:T(4,128)(2,1)S(1)} async-done(((bf16[4,8,4096]{2,0,1:T(4,128)(2,1)}), bf16[4,8,4096]{2,0,1:T(4,128)(2,1)S(1)}, u32[]{:S(2)}, u32[]{:S(2)}) %all-to-all-start.1) | async-done | bytes 262176 | tf_op jit(solution)/shard_map/all_to_all | solution.py:145
  188.5 0.3 copy.77
  188.8 0.1 reshape.162
  188.9 0.9 fusion
  (19 shorter events, 0.1 us)
Async XLA Ops:
  7.2 29.0 %copy-start = (bf16[256,4096]{1,0:T(8,128)(2,1)S(1)}, bf16[256,4096]{1,0:T(8,128)(2,1)}, u32[]{:S(2)}) copy-start(bf16[256,4096]{1,0:T(8,128)(2,1)} %param.31) | copy-start | bytes 6291460
  7.2 62.7 %reduce-scatter.6.cloned.1.call-start = ((), (), s32[]{:S(2)}) async-start(), calls=%async_computation.4 | async-start | bytes 589824 | tf_op jit(solution)/shard_map/reduce_scatter | solution.py:126
  27.2 6.6 %copy-start.6 = (f32[64,256]{1,0:T(8,128)S(1)}, f32[64,256]{1,0:T(8,128)}, u32[]{:S(2)}) copy-start(f32[64,256]{1,0:T(8,128)} %param.19) | copy-start | bytes 196612
  33.9 3.6 %copy-start.5 = (f32[64,256]{1,0:T(8,128)}, f32[64,256]{1,0:T(8,128)S(1)}, u32[]{:S(2)}) copy-start(f32[64,256]{1,0:T(8,128)S(1)} %fusion.29) | copy-start | bytes 196612
  36.1 1.4 copy-start.8
  36.1 2.1 %copy-start.7 = (bf16[4096]{0:T(1024)(128)(2,1)S(1)}, bf16[4096]{0:T(1024)(128)(2,1)}, u32[]{:S(2)}) copy-start(bf16[4096]{0:T(1024)(128)(2,1)} %param.32) | copy-start | bytes 24580
  36.1 2.1 %copy-start.10 = (u32[32]{0:T(128)S(1)}, u32[32]{0:T(128)}, u32[]{:S(2)}) copy-start(u32[32]{0:T(128)} %constant.63) | copy-start | bytes 388
  36.1 33.8 %copy-start.3 = (bf16[8,4096]{1,0:T(8,128)(2,1)S(1)}, bf16[8,4096]{1,0:T(8,128)(2,1)}, u32[]{:S(2)}) copy-start(bf16[8,4096]{1,0:T(8,128)(2,1)} %param.18) | copy-start | bytes 196612
  37.4 71.6 %all-gather.2.cloned.1.call-start = ((), (), s32[]{:S(2)}) async-start(), calls=%async_computation.5 | async-start | bytes 2359296 | tf_op jit(solution)/shard_map/all_gather | solution.py:140
  82.5 95.3 %reduce-scatter.8.cloned.1.call-start = ((), (), s32[]{:S(2)}) async-start(), calls=%async_computation.6 | async-start | bytes 2359296
  109.0 9.5 %copy-start.2 = (bf16[4,64,4096]{2,1,0:T(8,128)(2,1)S(1)}, bf16[4,64,4096]{2,1,0:T(8,128)(2,1)}, u32[]{:S(2)}) copy-start(bf16[4,64,4096]{2,1,0:T(8,128)(2,1)} %all-gather.2.cloned.1.call-done) | copy-start | bytes 6291460
  142.1 41.0 %slice-start = ((bf16[64,3,256]{2,0,1:T(8,128)(2,1)}), bf16[64,2,256]{2,0,1:T(8,128)(2,1)S(1)}, s32[]{:S(2)}) async-start(bf16[64,3,256]{2,0,1:T(8,128)(2,1)} %param.20), calls=%async_computation.7 | async-start | bytes 131072 | tf_op jit(solution)/shard_map/slice | solution.py:92
  142.1 41.6 %copy-start.9 = (f32[8,4]{0,1:T(4,128)S(1)}, f32[8,4]{0,1:T(4,128)}, u32[]{:S(2)}) copy-start(f32[8,4]{0,1:T(4,128)} %param.22) | copy-start | bytes 388
  142.1 47.6 %copy-start.1 = (bf16[256,4096]{1,0:T(8,128)(2,1)S(1)}, bf16[256,4096]{1,0:T(8,128)(2,1)}, u32[]{:S(2)}) copy-start(bf16[256,4096]{1,0:T(8,128)(2,1)} %param.31) | copy-start | bytes 6291460
  142.1 46.7 %copy-start.4 = (bf16[8,4096]{1,0:T(8,128)(2,1)S(1)}, bf16[8,4096]{1,0:T(8,128)(2,1)}, u32[]{:S(2)}) copy-start(bf16[8,4096]{1,0:T(8,128)(2,1)} %reduce-scatter.6.cloned.1.call-done) | copy-start | bytes 196612
  179.6 8.9 %all-to-all-start.1 = ((bf16[4,8,4096]{2,0,1:T(4,128)(2,1)}), bf16[4,8,4096]{2,0,1:T(4,128)(2,1)S(1)}, u32[]{:S(2)}, u32[]{:S(2)}) async-start(bf16[4,8,4096]{2,0,1:T(4,128)(2,1)} %bitcast.19), calls=%async_computation.2 | async-start | bytes 524288 | tf_op jit(solution)/shard_map/all_to_all | solution.py:145
Sparse Core Ops, SparseCore 0:
  37.6 32.2 reduce-scatter.5
  82.6 26.3 all-gather.1
  142.3 35.4 reduce-scatter.7
where the time goes:
time: 197 us; the launch traced here: 196 us
  waiting for transfers between devices  79.8 us (41%)
  blocking collectives  42.7 us (22%)
  matrix products  36.8 us (19%)
  between operations  14.6 us (7%)
  local copies, waits for them, and re-layouts  10.3 us (5%)
  other arithmetic  8.29 us (4%)
  starting transfers between devices  3.84 us (2%)
    unnamed x4, waiting for transfers between devices  35.6 us
    all_gather x1, waiting for transfers between devices, per_device(): lax.all_gather(arrived, 'tp', axis=1, tiled=True)  26.3 us
    dot_general x1, matrix products, run_experts(): jnp.einsum('erf,efd->erd', act, expert_down, preferred_element_type=jnp.f...  17.8 us
    unnamed x1, blocking collectives  17 us
    all_gather x1, blocking collectives, per_device(): piece = lax.all_gather(normed, 'tp', axis=0, tiled=True)  16.5 us
    reduce_scatter x1, waiting for transfers between devices, per_device(): lax.psum_scatter(partial_value.astype(jnp.bfloat16), 'tp', scatter_dimens...  13.2 us
    dot_general x1, matrix products, run_experts(): jnp.einsum('erd,edf->erf', piece, expert_gate, preferred_element_type=jnp...  9.51 us
    all_to_all x1, blocking collectives, per_device(): lax.all_to_all(outgoing, 'ep', split_axis=0, concat_axis=1, tiled=True)  9.19 us
  transfers between devices with their start and end apart: 4, of which 4 were waited for; matrix products, arithmetic and copies ran while one was open for 1% of the time, Pallas kernels for 0%

commit v1 on v0

--- a/solution.py
+++ b/solution.py
@@ -71,7 +71,12 @@
     first_channel = tp_place * local_width
     own_values = tokens.astype(jnp.float32)
     normed = norm_rows(own_values, first_gain).astype(jnp.bfloat16)
-    piece = lax.all_gather(normed, "tp", axis=0, tiled=True)
+    ring = [normed]
+    for hop in range(7):
+        ring.append(lax.ppermute(ring[-1], "tp", [(dev, (dev + 1) % 8) for dev in range(8)]))
+    piece = jnp.roll(
+        jnp.concatenate(ring[::-1], axis=0), (lax.axis_index("tp") + 1) * ring[0].shape[0], axis=0
+    )
     both = jnp.concatenate(
         [
             jnp.dot(piece, proj_input, preferred_element_type=jnp.float32),

time: 197 us -> 213 us (1.081)
  waiting for transfers between devices: 79.8 us -> 116 us
  blocking collectives: 42.7 us -> 22.9 us
  matrix products: 36.8 us -> 33.6 us
    ppermute x0 -> x7, waiting for transfers between devices: none -> 35.7 us  [per_device(): lax.ppermute(ring[-1], 'tp', [(dev, (dev + 1) % 8) for dev in range(8)])]
    all_gather x1 -> x0, blocking collectives: 16.5 us -> none  [per_device(): piece = lax.all_gather(normed, 'tp', axis=0, tiled=True)]
    unnamed x1, blocking collectives: 17 us -> 13.6 us
    unnamed x27 -> x45, local copies, waits for them, and re-layouts: 8.35 us -> 8.47 us
  transfers between devices with their start and end apart: 4 -> 11, of which waited for: 4 -> 11; matrix products, arithmetic and copies ran while one was open for 1% -> 3% of each run, Pallas kernels for 0% -> 0%
where the time goes in v1:
time: 213 us; the launch traced here: 212 us
  waiting for transfers between devices  116 us (54%)
  matrix products  33.6 us (16%)
  blocking collectives  22.9 us (11%)
  between operations  14.8 us (7%)
  local copies, waits for them, and re-layouts  10.4 us (5%)
  other arithmetic  9.25 us (4%)
  starting transfers between devices  4.56 us (2%)
    ppermute x7, waiting for transfers between devices, per_device(): lax.ppermute(ring[-1], 'tp', [(dev, (dev + 1) % 8) for dev in range(8)])  35.7 us
    unnamed x4, waiting for transfers between devices  35.6 us
    all_gather x1, waiting for transfers between devices, per_device(): lax.all_gather(arrived, 'tp', axis=1, tiled=True)  26.1 us
    dot_general x1, matrix products, run_experts(): jnp.einsum('erf,efd->erd', act, expert_down, preferred_element_type=jnp.f...  17.8 us
    reduce_scatter x1, waiting for transfers between devices, per_device(): lax.psum_scatter(partial_value.astype(jnp.bfloat16), 'tp', scatter_dimens...  14.4 us
    unnamed x1, blocking collectives  13.6 us
    dot_general x1, matrix products, run_experts(): jnp.einsum('erd,edf->erf', piece, expert_gate, preferred_element_type=jnp...  9.52 us
    all_to_all x1, blocking collectives, per_device(): lax.all_to_all(outgoing, 'ep', split_axis=0, concat_axis=1, tiled=True)  9.21 us
  transfers between devices with their start and end apart: 11, of which 11 were waited for; matrix products, arithmetic and copies ran while one was open for 3% of the time, Pallas kernels for 0%

profile of v1, /device:TPU:0, one launch (start us, length us, event | category | flops | bytes accessed | tf_op | source)
XLA Modules:
  0.0 211.9 jit_solution(6094531038213428651)
XLA Ops:
  7.2 0.0 copy-start
  7.2 0.0 reduce-scatter.6.cloned.1.call-start
  7.2 0.8 convert_element_type.98
  8.1 1.0 fusion.19
  9.1 0.9 fusion.21
  10.0 0.5 collective-permute-start
  10.6 6.0 %collective-permute-done = bf16[8,4096]{1,0:T(8,128)(2,1)S(1)} collective-permute-done((bf16[8,4096]{1,0:T(8,128)(2,1)S(1)}, bf16[8,4096]{1,0:T(8,128)(2,1)S(1)}, u32[]{:S(2)}, u32[]{:S(2)}) %collective-permute-start) | collective-permute-done | bytes 65568 | tf_op jit(solution)/shard_map/ppermute | solution.py:76
  16.5 5.5 %collective-permute-done.1 = bf16[8,4096]{1,0:T(8,128)(2,1)S(1)} collective-permute-done((bf16[8,4096]{1,0:T(8,128)(2,1)S(1)}, bf16[8,4096]{1,0:T(8,128)(2,1)S(1)}, u32[]{:S(2)}, u32[]{:S(2)}) %collective-permute-start.1) | collective-permute-done | bytes 65568 | tf_op jit(solution)/shard_map/ppermute | solution.py:76
  22.0 5.5 %collective-permute-done.2 = bf16[8,4096]{1,0:T(8,128)(2,1)S(1)} collective-permute-done((bf16[8,4096]{1,0:T(8,128)(2,1)S(1)}, bf16[8,4096]{1,0:T(8,128)(2,1)S(1)}, u32[]{:S(2)}, u32[]{:S(2)}) %collective-permute-start.2) | collective-permute-done | bytes 65568 | tf_op jit(solution)/shard_map/ppermute | solution.py:76
  27.5 0.7 dynamic-slice_convert_fusion
  28.2 4.8 %collective-permute-done.3 = bf16[8,4096]{1,0:T(8,128)(2,1)S(1)} collective-permute-done((bf16[8,4096]{1,0:T(8,128)(2,1)S(1)}, bf16[8,4096]{1,0:T(8,128)(2,1)S(1)}, u32[]{:S(2)}, u32[]{:S(2)}) %collective-permute-start.3) | collective-permute-done | bytes 65568 | tf_op jit(solution)/shard_map/ppermute | solution.py:76
  33.0 0.9 convert_element_type.101
  34.0 4.5 %collective-permute-done.4 = bf16[8,4096]{1,0:T(8,128)(2,1)S(1)} collective-permute-done((bf16[8,4096]{1,0:T(8,128)(2,1)S(1)}, bf16[8,4096]{1,0:T(8,128)(2,1)S(1)}, u32[]{:S(2)}, u32[]{:S(2)}) %collective-permute-start.4) | collective-permute-done | bytes 65568 | tf_op jit(solution)/shard_map/ppermute | solution.py:76
  38.5 0.8 fusion.59
  39.3 4.7 %collective-permute-done.5 = bf16[8,4096]{1,0:T(8,128)(2,1)S(1)} collective-permute-done((bf16[8,4096]{1,0:T(8,128)(2,1)S(1)}, bf16[8,4096]{1,0:T(8,128)(2,1)S(1)}, u32[]{:S(2)}, u32[]{:S(2)}) %collective-permute-start.5) | collective-permute-done | bytes 65568 | tf_op jit(solution)/shard_map/ppermute | solution.py:76
  44.0 0.8 dynamic-slice_convert_fusion.2
  44.7 4.7 %collective-permute-done.6 = bf16[8,4096]{1,0:T(8,128)(2,1)S(1)} collective-permute-done((bf16[8,4096]{1,0:T(8,128)(2,1)S(1)}, bf16[8,4096]{1,0:T(8,128)(2,1)S(1)}, u32[]{:S(2)}, u32[]{:S(2)}) %collective-permute-start.6) | collective-permute-done | bytes 65568 | tf_op jit(solution)/shard_map/ppermute | solution.py:76
  49.6 0.9 constant_dynamic-update-slice_fusion.8
  50.6 0.1 constant_dynamic-update-slice_fusion
  50.7 0.5 convolution_convert_fusion.4
  51.2 1.0 fusion.11
  52.3 1.0 fusion.7
  53.3 0.1 fusion.35
  53.4 0.6 multiply_reduce_fusion.1
  54.0 1.3 convolution_convert_fusion.1
  55.3 0.0 reduce-scatter.6.cloned.1.call-update
  55.3 0.0 all-gather.2.cloned.1.call-start
  55.4 0.1 constant_dynamic-slice_fusion
  55.4 0.1 copy.58
  55.5 0.1 eq.52
  55.6 0.1 fusion.53
  55.7 0.1 reduce_window_sum.11
  55.7 0.2 select_reduce_fusion.1
  55.9 0.1 reshape.160
  56.0 0.1 copy.50
  56.1 0.0 copy-done.12
  56.1 0.6 dynamic-slice
  57.4 0.1 fusion.54
  57.4 13.6 %all-reduce = bf16[64,1]{0,1:T(2,128)(2,1)S(1)} all-reduce(bf16[64,1]{0,1:T(2,128)(2,1)S(1)} %bitcast.95), channel_id=3, replica_groups=mesh['ep'=4,'tp'=8] {'tp'}, use_global_device_ids=true, to_apply=%region_3.4.clone | all-reduce | flops 64 | bytes 256
  71.1 0.1 rsqrt_bitcast_fusion
  71.2 14.4 %reduce-scatter.6.cloned.1.call-done = bf16[8,4096]{1,0:T(8,128)(2,1)} async-done(((bf16[64,4096]{1,0:T(8,128)(2,1)}), bf16[8,4096]{1,0:T(8,128)(2,1)}) %reduce-scatter.6.cloned.1.call-update) | async-done | bytes 65552 | tf_op jit(solution)/shard_map/reduce_scatter | solution.py:131
  85.5 1.1 multiply_reduce_fusion
  86.6 1.1 convolution_convert_fusion.2
  87.7 0.2 reshape.161
  87.9 9.2 %all_to_all.33 = bf16[16,2,4096]{2,1,0:T(2,128)(2,1)S(1)} all-to-all(bf16[16,2,4096]{2,1,0:T(2,128)(2,1)S(1)} %reshape.161), channel_id=1, replica_groups=mesh['ep'=4,'tp'=8] {'ep'}, dimensions={0} | all-to-all | bytes 524288 | tf_op jit(solution)/shard_map/all_to_all | solution.py:143
  97.1 0.2 copy.78
  97.3 0.8 all_to_all.27
  98.1 0.0 all-gather.2.cloned.1.call-update
  98.2 0.2 reduce-scatter.8.cloned.1.call-start
  98.4 26.1 %all-gather.2.cloned.1.call-done = bf16[4,64,4096]{2,1,0:T(8,128)(2,1)} async-done(((bf16[4,8,4096]{2,1,0:T(8,128)(2,1)}), bf16[4,64,4096]{2,1,0:T(8,128)(2,1)}) %all-gather.2.cloned.1.call-update) | async-done | bytes 2097168 | tf_op jit(solution)/shard_map/all_gather | solution.py:145
  124.5 9.5 %convolution_minimum_fusion = f32[4,64,512]{2,1,0:T(8,128)S(1)} fusion(bf16[4,64,4096]{2,1,0:T(8,128)(2,1)} %all-gather.2.cloned.1.call-done, bf16[4,4096,512]{2,1,0:T(8,128)(2,1)} %param.33), kind=kOutput, calls=%fused_computation.5 | convolution fusion | flops 1073872896 | bytes 19398656 | tf_op jit(solution)/shard_map/erd,edf->erf/dot_general | solution.py:35
  134.0 17.8 %convolution_convert_fusion = bf16[4,64,4096]{2,1,0:T(8,128)(2,1)} fusion(bf16[4,512,4096]{2,1,0:T(8,128)(2,1)} %param.35, bf16[4,64,4096]{2,1,0:T(8,128)(2,1)S(1)} %copy-done.2, bf16[4,4096,512]{2,1,0:T(8,128)(2,1)} %param.34, f32[4,64,512]{2,1,0:T(8,128)S(1)} %convolution_minimum_fusion), kind=kOutput, calls=%fused_computation | convolution fusion | flops 2149711872 | bytes 38273024 | tf_op jit(solution)/shard_map/erf,efd->erd/dot_general | solution.py:41
  151.8 3.2 %copy.56 = bf16[4,64,4096]{2,0,1:T(4,128)(2,1)S(1)} copy(bf16[4,64,4096]{2,1,0:T(8,128)(2,1)} %convolution_convert_fusion) | data formatting | bytes 4194304
  155.0 2.6 %copy.62 = bf16[8,8,4,4096]{3,1,2,0:T(8,128)(2,1)} copy(bf16[8,8,4,4096]{3,2,1,0:T(4,128)(2,1)S(1)} %bitcast.85) | data formatting | bytes 4194304
  157.6 0.0 reduce-scatter.8.cloned.1.call-update
  157.7 35.6 %reduce-scatter.8.cloned.1.call-done = bf16[8,16384]{1,0:T(8,128)(2,1)} async-done(((bf16[64,16384]{1,0:T(8,128)(2,1)}), bf16[8,16384]{1,0:T(8,128)(2,1)}) %reduce-scatter.8.cloned.1.call-update) | async-done | bytes 262160
  193.2 1.8 reshape.166
  195.1 3.7 %all-to-all-start.1 = ((bf16[4,8,4096]{2,0,1:T(4,128)(2,1)}), bf16[4,8,4096]{2,0,1:T(4,128)(2,1)S(1)}, u32[]{:S(2)}, u32[]{:S(2)}) async-start(bf16[4,8,4096]{2,0,1:T(4,128)(2,1)} %bitcast.19), calls=%async_computation.2 | async-start | bytes 524288 | tf_op jit(solution)/shard_map/all_to_all | solution.py:150
  198.8 0.1 select_reduce_fusion
  198.9 0.7 pad_maximum_fusion
  199.5 4.6 %all-to-all-done.1 = bf16[4,8,4096]{2,0,1:T(4,128)(2,1)S(1)} async-done(((bf16[4,8,4096]{2,0,1:T(4,128)(2,1)}), bf16[4,8,4096]{2,0,1:T(4,128)(2,1)S(1)}, u32[]{:S(2)}, u32[]{:S(2)}) %all-to-all-start.1) | async-done | bytes 262176 | tf_op jit(solution)/shard_map/all_to_all | solution.py:150
  204.1 0.3 copy.77
  204.4 0.1 reshape.162
  204.5 0.9 fusion
  (52 shorter events, 0.2 us)
Async XLA Ops:
  7.2 46.8 %copy-start = (bf16[256,4096]{1,0:T(8,128)(2,1)S(1)}, bf16[256,4096]{1,0:T(8,128)(2,1)}, u32[]{:S(2)}) copy-start(bf16[256,4096]{1,0:T(8,128)(2,1)} %param.31) | copy-start | bytes 6291460
  7.2 43.4 %copy-start.3 = (bf16[8,4096]{1,0:T(8,128)(2,1)S(1)}, bf16[8,4096]{1,0:T(8,128)(2,1)}, u32[]{:S(2)}) copy-start(bf16[8,4096]{1,0:T(8,128)(2,1)} %param.18) | copy-start | bytes 196612
  7.2 78.4 %reduce-scatter.6.cloned.1.call-start = ((), (), s32[]{:S(2)}) async-start(), calls=%async_computation.4 | async-start | bytes 589824 | tf_op jit(solution)/shard_map/reduce_scatter | solution.py:131
  10.0 6.5 %collective-permute-start = (bf16[8,4096]{1,0:T(8,128)(2,1)S(1)}, bf16[8,4096]{1,0:T(8,128)(2,1)S(1)}, u32[]{:S(2)}, u32[]{:S(2)}) collective-permute-start(bf16[8,4096]{1,0:T(8,128)(2,1)S(1)} %fusion.21), channel_id=1, source_target_pairs={{0,1},{1,2},{2,3},{3,4},{4,5},{5,6},{6,7},{7,0},{8,9},{9,10},{10,1... | collective-permute-start | bytes 196616 | tf_op jit(solution)/shard_map/ppermute | solution.py:76
  16.5 5.5 %collective-permute-start.1 = (bf16[8,4096]{1,0:T(8,128)(2,1)S(1)}, bf16[8,4096]{1,0:T(8,128)(2,1)S(1)}, u32[]{:S(2)}, u32[]{:S(2)}) collective-permute-start(bf16[8,4096]{1,0:T(8,128)(2,1)S(1)} %collective-permute-done), channel_id=1, source_target_pairs={{0,1},{1,2},{2,3},{3,4},{4,5},{5,6},{6,7},{7,0},{8,9},{9,10},{10,1... | collective-permute-start | bytes 196616 | tf_op jit(solution)/shard_map/ppermute | solution.py:76
  22.0 5.5 %collective-permute-start.2 = (bf16[8,4096]{1,0:T(8,128)(2,1)S(1)}, bf16[8,4096]{1,0:T(8,128)(2,1)S(1)}, u32[]{:S(2)}, u32[]{:S(2)}) collective-permute-start(bf16[8,4096]{1,0:T(8,128)(2,1)S(1)} %collective-permute-done.1), channel_id=1, source_target_pairs={{0,1},{1,2},{2,3},{3,4},{4,5},{5,6},{6,7},{7,0},{8,9},{9,10},{10,1... | collective-permute-start | bytes 196616 | tf_op jit(solution)/shard_map/ppermute | solution.py:76
  27.5 5.5 %collective-permute-start.3 = (bf16[8,4096]{1,0:T(8,128)(2,1)S(1)}, bf16[8,4096]{1,0:T(8,128)(2,1)S(1)}, u32[]{:S(2)}, u32[]{:S(2)}) collective-permute-start(bf16[8,4096]{1,0:T(8,128)(2,1)S(1)} %collective-permute-done.2), channel_id=1, source_target_pairs={{0,1},{1,2},{2,3},{3,4},{4,5},{5,6},{6,7},{7,0},{8,9},{9,10},{10,1... | collective-permute-start | bytes 196616 | tf_op jit(solution)/shard_map/ppermute | solution.py:76
  33.0 5.5 %collective-permute-start.4 = (bf16[8,4096]{1,0:T(8,128)(2,1)S(1)}, bf16[8,4096]{1,0:T(8,128)(2,1)S(1)}, u32[]{:S(2)}, u32[]{:S(2)}) collective-permute-start(bf16[8,4096]{1,0:T(8,128)(2,1)S(1)} %collective-permute-done.3), channel_id=1, source_target_pairs={{0,1},{1,2},{2,3},{3,4},{4,5},{5,6},{6,7},{7,0},{8,9},{9,10},{10,1... | collective-permute-start | bytes 196616 | tf_op jit(solution)/shard_map/ppermute | solution.py:76
  33.9 16.8 %copy-start.5 = (bf16[4096,256]{1,0:T(8,128)(2,1)S(1)}, bf16[4096,256]{1,0:T(8,128)(2,1)}, u32[]{:S(2)}) copy-start(bf16[4096,256]{1,0:T(8,128)(2,1)} %param.24) | copy-start | bytes 6291460
  38.5 5.5 %collective-permute-start.5 = (bf16[8,4096]{1,0:T(8,128)(2,1)S(1)}, bf16[8,4096]{1,0:T(8,128)(2,1)S(1)}, u32[]{:S(2)}, u32[]{:S(2)}) collective-permute-start(bf16[8,4096]{1,0:T(8,128)(2,1)S(1)} %collective-permute-done.4), channel_id=1, source_target_pairs={{0,1},{1,2},{2,3},{3,4},{4,5},{5,6},{6,7},{7,0},{8,9},{9,10},{10,1... | collective-permute-start | bytes 196616 | tf_op jit(solution)/shard_map/ppermute | solution.py:76
  44.0 5.5 %collective-permute-start.6 = (bf16[8,4096]{1,0:T(8,128)(2,1)S(1)}, bf16[8,4096]{1,0:T(8,128)(2,1)S(1)}, u32[]{:S(2)}, u32[]{:S(2)}) collective-permute-start(bf16[8,4096]{1,0:T(8,128)(2,1)S(1)} %collective-permute-done.5), channel_id=1, source_target_pairs={{0,1},{1,2},{2,3},{3,4},{4,5},{5,6},{6,7},{7,0},{8,9},{9,10},{10,1... | collective-permute-start | bytes 196616 | tf_op jit(solution)/shard_map/ppermute | solution.py:76
  50.5 2.7 %copy-start.8 = (f32[64,256]{1,0:T(8,128)S(1)}, f32[64,256]{1,0:T(8,128)}, u32[]{:S(2)}) copy-start(f32[64,256]{1,0:T(8,128)} %param.19) | copy-start | bytes 196612
  50.6 2.7 %copy-start.4 = (bf16[4096,256]{1,0:T(8,128)(2,1)S(1)}, bf16[4096,256]{1,0:T(8,128)(2,1)}, u32[]{:S(2)}) copy-start(bf16[4096,256]{1,0:T(8,128)(2,1)} %param.25) | copy-start | bytes 6291460
  53.4 1.9 copy-start.7
  53.9 1.4 copy-start.10
  54.0 2.1 %copy-start.9 = (bf16[4096]{0:T(1024)(128)(2,1)S(1)}, bf16[4096]{0:T(1024)(128)(2,1)}, u32[]{:S(2)}) copy-start(bf16[4096]{0:T(1024)(128)(2,1)} %param.32) | copy-start | bytes 24580
  54.0 2.1 %copy-start.12 = (u32[32]{0:T(128)S(1)}, u32[32]{0:T(128)}, u32[]{:S(2)}) copy-start(u32[32]{0:T(128)} %constant.85) | copy-start | bytes 388
  55.3 69.2 %all-gather.2.cloned.1.call-start = ((), (), s32[]{:S(2)}) async-start(), calls=%async_computation.5 | async-start | bytes 2359296 | tf_op jit(solution)/shard_map/all_gather | solution.py:145
  98.2 95.1 %reduce-scatter.8.cloned.1.call-start = ((), (), s32[]{:S(2)}) async-start(), calls=%async_computation.6 | async-start | bytes 2359296
  124.5 9.5 %copy-start.2 = (bf16[4,64,4096]{2,1,0:T(8,128)(2,1)S(1)}, bf16[4,64,4096]{2,1,0:T(8,128)(2,1)}, u32[]{:S(2)}) copy-start(bf16[4,64,4096]{2,1,0:T(8,128)(2,1)} %all-gather.2.cloned.1.call-done) | copy-start | bytes 6291460
  157.6 41.1 %copy-start.11 = (f32[8,4]{0,1:T(4,128)S(1)}, f32[8,4]{0,1:T(4,128)}, u32[]{:S(2)}) copy-start(f32[8,4]{0,1:T(4,128)} %param.22) | copy-start | bytes 388
  157.6 41.2 %slice-start = ((bf16[64,3,256]{2,0,1:T(8,128)(2,1)}), bf16[64,2,256]{2,0,1:T(8,128)(2,1)S(1)}, s32[]{:S(2)}) async-start(bf16[64,3,256]{2,0,1:T(8,128)(2,1)} %param.20), calls=%async_computation.7 | async-start | bytes 131072 | tf_op jit(solution)/shard_map/slice | solution.py:97
  157.6 47.8 %copy-start.1 = (bf16[256,4096]{1,0:T(8,128)(2,1)S(1)}, bf16[256,4096]{1,0:T(8,128)(2,1)}, u32[]{:S(2)}) copy-start(bf16[256,4096]{1,0:T(8,128)(2,1)} %param.31) | copy-start | bytes 6291460
  157.6 46.9 %copy-start.6 = (bf16[8,4096]{1,0:T(8,128)(2,1)S(1)}, bf16[8,4096]{1,0:T(8,128)(2,1)}, u32[]{:S(2)}) copy-start(bf16[8,4096]{1,0:T(8,128)(2,1)} %reduce-scatter.6.cloned.1.call-done) | copy-start | bytes 196612
  195.1 9.1 %all-to-all-start.1 = ((bf16[4,8,4096]{2,0,1:T(4,128)(2,1)}), bf16[4,8,4096]{2,0,1:T(4,128)(2,1)S(1)}, u32[]{:S(2)}, u32[]{:S(2)}) async-start(bf16[4,8,4096]{2,0,1:T(4,128)(2,1)} %bitcast.19), calls=%async_computation.2 | async-start | bytes 524288 | tf_op jit(solution)/shard_map/all_to_all | solution.py:150
Sparse Core Ops, SparseCore 0:
  55.4 30.0 reduce-scatter.5
  98.3 26.1 all-gather.1
  157.8 35.4 reduce-scatter.7
